TPU v7x, 32 devices: a whole 2x2x4 slice. The times are simulated.
32 devices in a mesh: sp: 8 (over z, core), tp: 4 (over y, x).
Axes of the slice: x: 2, y: 2, z: 4, core: 2. Of those that a mesh axis runs over, the one named last changes fastest.
Arguments:
- stream: bfloat16 [1024, 2048], P('sp'), may hold values from -6 to 6
- query_small: bfloat16 [1024, 1024], P('sp', 'tp'), may hold values from -6 to 6
- key_small: bfloat16 [1024, 1024], P('sp', 'tp'), may hold values from -6 to 6
- value_small: bfloat16 [1024, 1024], P('sp', 'tp'), may hold values from -6 to 6
- query_large: bfloat16 [1024, 2048], P('sp', 'tp'), may hold values from -6 to 6
- key_large: bfloat16 [1024, 2048], P('sp', 'tp'), may hold values from -6 to 6
- value_large: bfloat16 [1024, 2048], P('sp', 'tp'), may hold values from -6 to 6
- key_bias: bfloat16 [1024, 2, 16], P('sp', None, 'tp'), may hold values from -16 to 1
- out_small: bfloat16 [1024, 2048], P('tp'), may hold values from -0.75 to 0.75
- out_large: bfloat16 [2048, 2048], P('tp'), may hold values from -0.75 to 0.75
- gain_one: float32 [2048], replicated, may hold values from 0.1 to 1.9
- shift_one: float32 [2048], replicated, may hold values from -1.5 to 1.5
- gain_two: float32 [2048], replicated, may hold values from 0.1 to 1.9
- shift_two: float32 [2048], replicated, may hold values from -1.5 to 1.5
- expert_pick: int32 [1024, 2], P('sp'), may hold values from 0 to 7, as said below
- route_weight: float32 [1024, 2], P('sp'), may hold values from 0.2 to 1
- w_gate: bfloat16 [8, 2048, 4096], P('sp', None, 'tp'), may hold values from -0.125 to 0.125
- w_up: bfloat16 [8, 2048, 4096], P('sp', None, 'tp'), may hold values from -0.125 to 0.125
- w_down: bfloat16 [8, 4096, 2048], P('sp', 'tp'), may hold values from -0.09375 to 0.09375
Outputs:
- result: bfloat16 [1024, 2048], P(('sp', 'tp'))
Inputs may be any that keep to these rules, and one draw needn't show every extreme that they name: In each aligned block of 128 positions (the positions of one index of sp), no expert is named more than 64 times, and in every block some expert is named exactly 64 times. The two experts of a position differ and lie in one group: equal values of expert_pick // 2.
All inputs are finite; a program needn't handle non-finite values.
Results may differ from a plain program's by a relative error of at most 0.017.
Values may be sent and summed in bfloat16 or wider, within the bound.
A program may use at most 64 MiB of HBM per device.

v0:
```python
import jax
import jax.numpy as jnp
from jax import lax
from jax.sharding import PartitionSpec as P

HEAD_SMALL = 64
HEAD_LARGE = 128
ALPHA_RES = 2.0**0.25
NORM_EPS = 1e-05


def layer_norm(inputs, gain_vec, shift_vec):
    average = jnp.mean(inputs, axis=-1, keepdims=True)
    centred = inputs - average
    variance = jnp.mean(centred * centred, axis=-1, keepdims=True)
    return centred * lax.rsqrt(variance + NORM_EPS) * gain_vec + shift_vec


def stick_group(queries, key_rows, value_rows, log_bias, position):
    query_count = queries.shape[0]
    head_count = queries.shape[1]
    value_size = value_rows.shape[2]
    key_span = 4 * query_count
    score_scale = queries.shape[2] ** (-0.5)
    query_pos = position * query_count + jnp.arange(query_count, dtype=jnp.int32)
    block_count = (position * query_count + query_count + key_span - 1) // key_span

    def visit_block(turn_index, carry):
        running, stay_sum = carry
        first_key = (block_count - 1 - turn_index) * key_span
        key_block = lax.dynamic_slice_in_dim(key_rows, first_key, key_span, 0)
        value_block = lax.dynamic_slice_in_dim(value_rows, first_key, key_span, 0)
        bias_block = lax.dynamic_slice_in_dim(log_bias, first_key, key_span, 0).astype(jnp.float32)
        scores = jnp.einsum("qhd,khd->hqk", queries, key_block, preferred_element_type=jnp.float32)
        scores = scores * score_scale + bias_block.T[:, None, :]
        key_pos = first_key + jnp.arange(key_span, dtype=jnp.int32)
        causal = (key_pos[None, :] < query_pos[:, None])[None]
        log_stay = jnp.where(causal, jax.nn.log_sigmoid(-scores), 0.0)
        later_sum = lax.cumsum(log_stay, axis=2, reverse=True) - log_stay + stay_sum[:, :, None]
        stick_weight = jnp.where(
            causal, jnp.exp(jax.nn.log_sigmoid(scores) + later_sum), 0.0
        ).astype(jnp.bfloat16)
        running = running + jnp.einsum(
            "hqk,khd->qhd", stick_weight, value_block, preferred_element_type=jnp.float32
        )
        stay_sum = stay_sum + jnp.sum(log_stay, axis=2)
        return (running, stay_sum)

    start_total = jnp.zeros((query_count, head_count, value_size), jnp.float32)
    start_stay = jnp.zeros((head_count, query_count), jnp.float32)
    running, stay_sum = lax.fori_loop(0, block_count, visit_block, (start_total, start_stay))
    return running.reshape(query_count, head_count * value_size).astype(jnp.bfloat16)


def split_heads(array, head_size):
    return array.reshape(array.shape[0], array.shape[1] // head_size, head_size)


def local(
    stream,
    query_small,
    key_small,
    value_small,
    query_large,
    key_large,
    value_large,
    key_bias,
    out_small,
    out_large,
    gain_one,
    shift_one,
    gain_two,
    shift_two,
    expert_pick,
    route_weight,
    w_gate,
    w_up,
    w_down,
):
    row_count = stream.shape[0]
    position = lax.axis_index("sp")
    gathered = (
        lax.all_gather(key_small, "sp", axis=0, tiled=True),
        lax.all_gather(value_small, "sp", axis=0, tiled=True),
        lax.all_gather(key_large, "sp", axis=0, tiled=True),
        lax.all_gather(value_large, "sp", axis=0, tiled=True),
        lax.all_gather(key_bias, "sp", axis=0, tiled=True),
    )
    att_small = stick_group(
        split_heads(query_small, HEAD_SMALL),
        split_heads(gathered[0], HEAD_SMALL),
        split_heads(gathered[1], HEAD_SMALL),
        gathered[4][:, 0],
        position,
    )
    att_large = stick_group(
        split_heads(query_large, HEAD_LARGE),
        split_heads(gathered[2], HEAD_LARGE),
        split_heads(gathered[3], HEAD_LARGE),
        gathered[4][:, 1],
        position,
    )
    partial_value = jnp.dot(att_small, out_small, preferred_element_type=jnp.float32)
    partial_value = partial_value + jnp.dot(
        att_large, out_large, preferred_element_type=jnp.float32
    )
    mixer_out = lax.psum(partial_value.astype(jnp.bfloat16), "tp").astype(jnp.float32)
    normed = layer_norm(
        ALPHA_RES * stream.astype(jnp.float32) + mixer_out, gain_one, shift_one
    ).astype(jnp.bfloat16)
    experts = w_gate.shape[0] * lax.axis_size("sp")
    capacity = 4 * row_count // experts
    tp_count = lax.axis_size("tp")
    tp_index = lax.axis_index("tp")
    per_lane = capacity // tp_count
    flat_picks = expert_pick.reshape(-1)
    one_hot = (flat_picks[:, None] == jnp.arange(experts, dtype=jnp.int32)[None, :]).astype(
        jnp.int32
    )
    slot_rank = jnp.sum((jnp.cumsum(one_hot, axis=0) - one_hot) * one_hot, axis=1)
    slot_index = (flat_picks * capacity + slot_rank).reshape(row_count, 2)

    def selector(first_slot, slot_count):
        target = (
            jnp.arange(experts, dtype=jnp.int32)[:, None] * capacity
            + first_slot
            + jnp.arange(slot_count, dtype=jnp.int32)[None, :]
        ).reshape(-1)
        return [target[:, None] == slot_index[None, :, pick_index] for pick_index in range(2)]

    own_select = selector(tp_index * per_lane, per_lane)
    all_select = selector(0, capacity)
    placing = (all_select[0] | all_select[1]).astype(jnp.bfloat16)
    outgoing = jnp.dot(placing, normed, preferred_element_type=jnp.float32).astype(jnp.bfloat16)
    arrived = lax.all_to_all(
        outgoing.reshape(experts, capacity, normed.shape[1]),
        "sp",
        split_axis=0,
        concat_axis=0,
        tiled=True,
    )
    flat_rows = arrived.reshape(-1, arrived.shape[2])
    gate = jnp.dot(flat_rows, w_gate[0], preferred_element_type=jnp.float32)
    upper = jnp.dot(flat_rows, w_up[0], preferred_element_type=jnp.float32)
    hidden = (jax.nn.silu(gate) * upper).astype(jnp.bfloat16)
    expert_terms = jnp.dot(hidden, w_down[0], preferred_element_type=jnp.float32).reshape(
        arrived.shape
    )
    summed = lax.psum_scatter(
        expert_terms.astype(jnp.bfloat16), "tp", scatter_dimension=1, tiled=True
    )
    returned = lax.all_to_all(summed, "sp", split_axis=0, concat_axis=0, tiled=True).reshape(
        experts * per_lane, normed.shape[1]
    )
    picked_first = jnp.einsum(
        "sr,sd->rd",
        own_select[0].astype(jnp.bfloat16),
        returned,
        preferred_element_type=jnp.float32,
    )
    picked_second = jnp.einsum(
        "sr,sd->rd",
        own_select[1].astype(jnp.bfloat16),
        returned,
        preferred_element_type=jnp.float32,
    )
    partial_mix = route_weight[:, 0:1] * picked_first + route_weight[:, 1:2] * picked_second
    expert_mix = lax.psum_scatter(
        partial_mix.astype(jnp.bfloat16), "tp", scatter_dimension=0, tiled=True
    ).astype(jnp.float32)
    own_count = row_count // tp_count
    own_rows = lax.dynamic_slice_in_dim(normed, tp_index * own_count, own_count, 0).astype(
        jnp.float32
    )
    return layer_norm(ALPHA_RES * own_rows + expert_mix, gain_two, shift_two).astype(jnp.bfloat16)


def solution(mesh):
    placed = (
        P("sp", None),
        P("sp", "tp"),
        P("sp", "tp"),
        P("sp", "tp"),
        P("sp", "tp"),
        P("sp", "tp"),
        P("sp", "tp"),
        P("sp", None, "tp"),
        P("tp", None),
        P("tp", None),
        P(),
        P(),
        P(),
        P(),
        P("sp", None),
        P("sp", None),
        P("sp", None, "tp"),
        P("sp", None, "tp"),
        P("sp", "tp", None),
    )
    return jax.shard_map(
        local, mesh=mesh, in_specs=placed, out_specs=P(("sp", "tp"), None), check_vma=False
    )
```

profile of v0, /device:TPU:0, one launch (start us, length us, event | category | flops | bytes accessed | tf_op | source)
XLA Modules:
  0.0 308.8 jit_solution(16901779927208205909)
XLA Ops:
  7.3 1.7 copy.76
  9.1 13.8 %all_gather.17 = bf16[1024,2,4]{0,2,1:T(4,128)(2,1)S(1)} all-gather(bf16[128,2,4]{0,2,1:T(4,128)(2,1)} %param.30), channel_id=1, replica_groups=mesh['sp'=8,'tp'=4] {'sp'}, dimensions={0}, use_global_device_ids=true | all-gather | bytes 18432 | tf_op jit(solution)/shard_map/all_gather | solution.py:87
  23.9 16.5 %all_gather.16 = bf16[1024,256]{1,0:T(8,128)(2,1)S(1)} all-gather(bf16[128,256]{1,0:T(8,128)(2,1)} %param.25), channel_id=1, replica_groups=mesh['sp'=8,'tp'=4] {'sp'}, dimensions={0}, use_global_device_ids=true | all-gather | bytes 589824 | tf_op jit(solution)/shard_map/all_gather | solution.py:83
  40.5 16.8 %all_gather.15 = bf16[1024,256]{1,0:T(8,128)(2,1)S(1)} all-gather(bf16[128,256]{1,0:T(8,128)(2,1)S(1)} %copy-done.12), channel_id=1, replica_groups=mesh['sp'=8,'tp'=4] {'sp'}, dimensions={0}, use_global_device_ids=true | all-gather | bytes 589824 | tf_op jit(solution)/shard_map/all_gather | solution.py:84
  58.3 10.1 %while.30 = (s32[]{:T(128)}, f32[128,4,64]{0,2,1:T(8,128)S(1)}, f32[4,128]{1,0:T(4,128)S(1)}, s32[]{:T(128)}, s32[]{:T(128)}, /*index=5*/bf16[1024,4,64]{0,2,1:T...) while((s32[]{:T(128)}, f32[128,4,64]{0,2,1:T(8,128)S(1)}, ...), condition=%wide.region_4.5_spmd.clone, body=%wide.region_0.4_spmd.clone.sunk | while | flops 109160584 | bytes 23688592 | solution.py:51
  58.6 2.0 fusion.106
  60.5 4.8 %fusion.107 = f32[4,128,4,128]{1,2,3,0:T(4,128)S(1)} fusion(f32[4,128,4,128]{1,3,2,0:T(8,128)S(1)} %bitcast.122), kind=kOutput, calls=%fused_computation.18.clone.1 | output fusion | flops 33292288 | bytes 2097152 | tf_op jit(solution)/shard_map/reduce-window.10
  66.6 1.5 fusion.108
  70.1 2.6 fusion.71
  72.7 2.3 copy.75
  75.0 11.4 %while.31 = (s32[]{:T(128)}, f32[128,4,128]{0,2,1:T(8,128)S(1)}, f32[4,128]{1,0:T(4,128)S(1)}, s32[]{:T(128)}, s32[]{:T(128)}, /*index=5*/bf16[1024,4,128]{0,2,1...) while((s32[]{:T(128)}, f32[128,4,128]{0,2,1:T(8,128)S(1)}, ...), condition=%wide.region_9.10_spmd.clone, body=%wide.region_5.9_spmd.clone.sunk | while | flops 176302208 | bytes 22967640 | solution.py:51
  75.4 3.1 fusion.114
  78.4 4.8 %fusion.115 = f32[4,128,4,128]{1,2,3,0:T(4,128)S(1)} fusion(f32[4,128,4,128]{1,3,2,0:T(8,128)S(1)} %bitcast.123), kind=kOutput, calls=%fused_computation.47.clone.1 | output fusion | flops 33292288 | bytes 2097152 | tf_op jit(solution)/shard_map/reduce-window.12
  86.4 2.5 fusion.50
  89.4 64.7 %all-reduce.2.cloned.1.call-done = bf16[128,2048]{1,0:T(8,128)(2,1)} async-done(((bf16[128,2048]{1,0:T(8,128)(2,1)}), bf16[128,2048]{1,0:T(8,128)(2,1)}) %all-reduce.2.cloned.1.call-update) | async-done | bytes 524304 | tf_op jit(solution)/shard_map/psum | solution.py:107
  157.9 53.7 %all_to_all.10 = bf16[8,64,2048]{2,1,0:T(8,128)(2,1)S(1)} all-to-all(bf16[8,64,2048]{2,1,0:T(8,128)(2,1)S(1)} %bitcast.125), channel_id=1, replica_groups=mesh['sp'=8,'tp'=4] {'sp'}, dimensions={0} | all-to-all | bytes 4194304 | tf_op jit(solution)/shard_map/all_to_all | solution.py:135
  211.7 2.3 fusion.44
  214.0 2.5 multiply_convert_fusion
  216.6 3.7 %fusion.46 = bf16[8,64,2048]{2,1,0:T(8,128)(2,1)} fusion(bf16[8,64,1024]{2,1,0:T(8,128)(2,1)S(1)} %bitcast.137, bf16[1,1024,2048]{2,1,0:T(8,128)(2,1)S(1)} %copy-done.24), kind=kOutput, calls=%fused_computation.66 | convolution fusion | flops 2148532224 | bytes 7340032 | tf_op jit(solution)/shard_map/dot_general | solution.py:146
  220.3 33.3 %reduce-scatter.3.cloned.1.call-done = bf16[8,16,2048]{2,1,0:T(8,128)(2,1)} async-done(((bf16[8,64,2048]{2,1,0:T(8,128)(2,1)}), bf16[8,16,2048]{2,1,0:T(8,128)(2,1)}) %reduce-scatter.3.cloned.1.call-update) | async-done | bytes 524304 | tf_op jit(solution)/shard_map/reduce_scatter | solution.py:149
  253.6 4.6 %all-to-all-start.1 = ((bf16[8,16,2048]{2,1,0:T(8,128)(2,1)}), bf16[8,16,2048]{2,1,0:T(8,128)(2,1)S(1)}, u32[]{:S(2)}, u32[]{:S(2)}) async-start(bf16[8,16,2048]{2,1,0:T(8,128)(2,1)} %reduce-scatter.3.cloned.1.call-done), calls=%async_computation.2 | async-start | bytes 1048576 | tf_op jit(solution)/shard_map/all_to_all | solution.py:152
  258.4 15.1 %all-to-all-done.1 = bf16[8,16,2048]{2,1,0:T(8,128)(2,1)S(1)} async-done(((bf16[8,16,2048]{2,1,0:T(8,128)(2,1)}), bf16[8,16,2048]{2,1,0:T(8,128)(2,1)S(1)}, u32[]{:S(2)}, u32[]{:S(2)}) %all-to-all-start.1) | async-done | bytes 524320 | tf_op jit(solution)/shard_map/all_to_all | solution.py:152
  275.2 23.2 %reduce-scatter.5.cloned.1.call-done = bf16[32,2048]{1,0:T(8,128)(2,1)} async-done(((bf16[128,2048]{1,0:T(8,128)(2,1)}), bf16[32,2048]{1,0:T(8,128)(2,1)}) %reduce-scatter.5.cloned.1.call-update) | async-done | bytes 131088 | tf_op jit(solution)/shard_map/reduce_scatter | solution.py:168
  300.6 1.7 add_convert_fusion.1
  (130 shorter events, 17.8 us)
Async XLA Ops:
  6.5 79.8 %copy-start = (bf16[512,2048]{1,0:T(8,128)(2,1)S(1)}, bf16[512,2048]{1,0:T(8,128)(2,1)}, u32[]{:S(2)}) copy-start(bf16[512,2048]{1,0:T(8,128)(2,1)} %param.32) | copy-start | bytes 6291460
  6.5 34.0 %copy-start.12 = (bf16[128,256]{1,0:T(8,128)(2,1)S(1)}, bf16[128,256]{1,0:T(8,128)(2,1)}, u32[]{:S(2)}) copy-start(bf16[128,256]{1,0:T(8,128)(2,1)} %param.26) | copy-start | bytes 196612
  6.5 66.1 %all-gather.3.cloned.1.call-start = ((), (), s32[]{:S(2)}) async-start(), calls=%async_computation.4 | async-start | bytes 1179648 | tf_op jit(solution)/shard_map/all_gather | solution.py:86
  7.3 67.7 %all-gather.5.cloned.1.call-start = ((), (), s32[]{:S(2)}) async-start(), calls=%async_computation.5 | async-start | bytes 1179648 | tf_op jit(solution)/shard_map/all_gather | solution.py:85
  9.0 145.1 %all-reduce.2.cloned.1.call-start = ((), (), s32[]{:S(2)}) async-start(), calls=%async_computation.6 | async-start | bytes 1048576 | tf_op jit(solution)/shard_map/psum | solution.py:107
  58.3 10.1 %copy-start.20 = (s32[128,2]{0,1:T(2,128)S(1)}, s32[128,2]{0,1:T(2,128)}, u32[]{:S(2)}) copy-start(s32[128,2]{0,1:T(2,128)} %param.37) | copy-start | bytes 3076
  58.3 11.5 %copy-start.9 = (bf16[128,512]{1,0:T(8,128)(2,1)S(1)}, bf16[128,512]{1,0:T(8,128)(2,1)}, u32[]{:S(2)}) copy-start(bf16[128,512]{1,0:T(8,128)(2,1)} %param.27) | copy-start | bytes 393220
  65.6 2.5 copy-start.4
  69.8 5.1 %copy-start.19 = (s32[8,3]{0,1:T(4,128)}, s32[8,3]{0,1:T(4,128)S(1)}, u32[]{:S(2)}) copy-start(s32[8,3]{0,1:T(4,128)S(1)} %reduce-window.39) | copy-start | bytes 292
  75.2 3.3 %copy-start.10 = (bf16[128,4,128]{2,0,1:T(8,128)(2,1)}, bf16[128,4,128]{2,0,1:T(8,128)(2,1)S(1)}, u32[]{:S(2)}) copy-start(bf16[128,4,128]{2,0,1:T(8,128)(2,1)S(1)} %get-tuple-element.581) | copy-start | bytes 393220 | tf_op jit(solution)/shard_map/while
  83.5 2.5 copy-start.3
  86.4 2.6 slice-start
  86.4 67.7 %copy-start.5 = (bf16[128,2048]{1,0:T(8,128)(2,1)S(1)}, bf16[128,2048]{1,0:T(8,128)(2,1)}, u32[]{:S(2)}) copy-start(bf16[128,2048]{1,0:T(8,128)(2,1)} %param.23) | copy-start | bytes 1572868
  88.9 67.9 %copy-start.15 = (f32[2048]{0:T(1024)S(1)}, f32[2048]{0:T(1024)}, u32[]{:S(2)}) copy-start(f32[2048]{0:T(1024)} %param.34) | copy-start | bytes 24580
  89.0 67.9 %copy-start.16 = (f32[2048]{0:T(1024)S(1)}, f32[2048]{0:T(1024)}, u32[]{:S(2)}) copy-start(f32[2048]{0:T(1024)} %param.33) | copy-start | bytes 24580
  89.0 164.6 %reduce-scatter.3.cloned.1.call-start = ((), (), s32[]{:S(2)}) async-start(), calls=%async_computation.7 | async-start | bytes 2621440 | tf_op jit(solution)/shard_map/reduce_scatter | solution.py:149
  154.1 2.8 copy-start.6
  157.9 53.7 %copy-start.22 = (bf16[1,2048,1024]{2,1,0:T(8,128)(2,1)S(1)}, bf16[1,2048,1024]{2,1,0:T(8,128)(2,1)}, u32[]{:S(2)}) copy-start(bf16[1,2048,1024]{2,1,0:T(8,128)(2,1)} %param.39) | copy-start | bytes 12582916
  214.0 2.5 copy-start.24
  220.3 38.1 %copy-start.21 = (f32[128,2]{0,1:T(2,128)S(1)}, f32[128,2]{0,1:T(2,128)}, u32[]{:S(2)}) copy-start(f32[128,2]{0,1:T(2,128)} %param.38) | copy-start | bytes 3076
  253.6 19.9 %all-to-all-start.1 = ((bf16[8,16,2048]{2,1,0:T(8,128)(2,1)}), bf16[8,16,2048]{2,1,0:T(8,128)(2,1)S(1)}, u32[]{:S(2)}, u32[]{:S(2)}) async-start(bf16[8,16,2048]{2,1,0:T(8,128)(2,1)} %reduce-scatter.3.cloned.1.call-done), calls=%async_computation.2 | async-start | bytes 1048576 | tf_op jit(solution)/shard_map/all_to_all | solution.py:152
  258.2 40.2 %reduce-scatter.5.cloned.1.call-start = ((), (), s32[]{:S(2)}) async-start(), calls=%async_computation.8 | async-start | bytes 655360 | tf_op jit(solution)/shard_map/reduce_scatter | solution.py:168
  273.5 27.0 %copy-start.17 = (f32[2048]{0:T(1024)S(1)}, f32[2048]{0:T(1024)}, u32[]{:S(2)}) copy-start(f32[2048]{0:T(1024)} %param.36) | copy-start | bytes 24580
  273.5 27.1 %copy-start.18 = (f32[2048]{0:T(1024)S(1)}, f32[2048]{0:T(1024)}, u32[]{:S(2)}) copy-start(f32[2048]{0:T(1024)} %param.35) | copy-start | bytes 24580
  (8 other events, 14.5 us)
Sparse Core Ops, SparseCore 0:
  8.9 27.5 all-gather.2
  38.1 26.5 all-gather.4
  89.1 64.9 all-reduce.1
  220.4 33.1 reduce-scatter.2
  275.3 23.0 reduce-scatter.4
where the time goes:
time: 309 us
  waiting for transfers between devices  137 us (44%)
  blocking collectives  101 us (33%)
  matrix products  21.6 us (7%)
  other arithmetic  21.1 us (7%)
  between operations  13.4 us (4%)
  local copies, waits for them, and re-layouts  9.51 us (3%)
  starting transfers between devices  4.77 us (2%)
    psum x1, waiting for transfers between devices, local(): lax.psum(partial_value.astype(jnp.bfloat16), 'tp').astype(jnp.float32)  64.7 us
    all_to_all x1, blocking collectives, local(): lax.all_to_all(outgoing.reshape(experts, capacity, normed.shape[1]), 'sp'...  53.7 us
    reduce_scatter x1, waiting for transfers between devices, local(): lax.psum_scatter(expert_terms.astype(jnp.bfloat16), 'tp', scatter_dimensi...  33.3 us
    reduce_scatter x1, waiting for transfers between devices, local(): lax.psum_scatter(partial_mix.astype(jnp.bfloat16), 'tp', scatter_dimensio...  23.2 us
    all_gather x1, blocking collectives, local(): lax.all_gather(value_small, 'sp', axis=0, tiled=True)  16.8 us
    all_gather x1, blocking collectives, local(): lax.all_gather(key_small, 'sp', axis=0, tiled=True)  16.5 us
    all_to_all x1, waiting for transfers between devices, local(): lax.all_to_all(summed, 'sp', split_axis=0, concat_axis=0, tiled=True)  15.1 us
    all_gather x1, blocking collectives, local(): lax.all_gather(key_bias, 'sp', axis=0, tiled=True)  13.8 us
  transfers between devices with their start and end apart: 6, of which 4 were waited for; matrix products, arithmetic and copies ran while one was open for 6% of the time, Pallas kernels for 0%

commit v1 on v0

--- a/solution.py
+++ b/solution.py
@@ -104,7 +104,9 @@
     partial_value = partial_value + jnp.dot(
         att_large, out_large, preferred_element_type=jnp.float32
     )
-    mixer_out = lax.psum(partial_value.astype(jnp.bfloat16), "tp").astype(jnp.float32)
+    mixer_out = jnp.sum(lax.all_gather(partial_value.astype(jnp.bfloat16), "tp"), axis=0).astype(
+        jnp.float32
+    )
     normed = layer_norm(
         ALPHA_RES * stream.astype(jnp.float32) + mixer_out, gain_one, shift_one
     ).astype(jnp.bfloat16)

time: 309 us -> 298 us (0.964)
  waiting for transfers between devices: 137 us -> 126 us
    psum x1 -> x0, waiting for transfers between devices: 64.7 us -> none  [local(): lax.psum(partial_value.astype(jnp.bfloat16), 'tp').astype(jnp.float32)]
    all_gather x0 -> x1, waiting for transfers between devices: none -> 53.1 us  [local(): lax.all_gather(partial_value.astype(jnp.bfloat16), 'tp')]
  transfers between devices with their start and end apart: 6 -> 6, of which waited for: 4 -> 4; matrix products, arithmetic and copies ran while one was open for 6% -> 7% of each run, Pallas kernels for 0% -> 0%
where the time goes in v1:
time: 298 us; the launch traced here: 297 us
  waiting for transfers between devices  126 us (42%)
  blocking collectives  101 us (34%)
  matrix products  21.5 us (7%)
  other arithmetic  21.1 us (7%)
  between operations  13.4 us (4%)
  local copies, waits for them, and re-layouts  9.5 us (3%)
  starting transfers between devices  4.77 us (2%)
    all_to_all x1, blocking collectives, local(): lax.all_to_all(outgoing.reshape(experts, capacity, normed.shape[1]), 'sp'...  53.7 us
    all_gather x1, waiting for transfers between devices, local(): lax.all_gather(partial_value.astype(jnp.bfloat16), 'tp')  53.1 us
    reduce_scatter x1, waiting for transfers between devices, local(): lax.psum_scatter(expert_terms.astype(jnp.bfloat16), 'tp', scatter_dimensi...  33.3 us
    reduce_scatter x1, waiting for transfers between devices, local(): lax.psum_scatter(partial_mix.astype(jnp.bfloat16), 'tp', scatter_dimensio...  23.2 us
    all_gather x1, blocking collectives, local(): lax.all_gather(value_small, 'sp', axis=0, tiled=True)  16.8 us
    all_gather x1, blocking collectives, local(): lax.all_gather(key_small, 'sp', axis=0, tiled=True)  16.5 us
    all_to_all x1, waiting for transfers between devices, local(): lax.all_to_all(summed, 'sp', split_axis=0, concat_axis=0, tiled=True)  15.1 us
    all_gather x1, blocking collectives, local(): lax.all_gather(key_bias, 'sp', axis=0, tiled=True)  13.8 us
  transfers between devices with their start and end apart: 6, of which 4 were waited for; matrix products, arithmetic and copies ran while one was open for 7% of the time, Pallas kernels for 0%

profile of v1, /device:TPU:0, one launch (start us, length us, event | category | flops | bytes accessed | tf_op | source)
XLA Modules:
  0.0 297.1 jit_solution(13738786449857121244)
XLA Ops:
  7.3 1.7 copy.76
  9.1 13.8 %all_gather.23 = bf16[1024,2,4]{0,2,1:T(4,128)(2,1)S(1)} all-gather(bf16[128,2,4]{0,2,1:T(4,128)(2,1)} %param.30), channel_id=1, replica_groups=mesh['sp'=8,'tp'=4] {'sp'}, dimensions={0}, use_global_device_ids=true | all-gather | bytes 18432 | tf_op jit(solution)/shard_map/all_gather | solution.py:87
  23.9 16.5 %all_gather.22 = bf16[1024,256]{1,0:T(8,128)(2,1)S(1)} all-gather(bf16[128,256]{1,0:T(8,128)(2,1)} %param.25), channel_id=1, replica_groups=mesh['sp'=8,'tp'=4] {'sp'}, dimensions={0}, use_global_device_ids=true | all-gather | bytes 589824 | tf_op jit(solution)/shard_map/all_gather | solution.py:83
  40.5 16.8 %all_gather.21 = bf16[1024,256]{1,0:T(8,128)(2,1)S(1)} all-gather(bf16[128,256]{1,0:T(8,128)(2,1)S(1)} %copy-done.13), channel_id=1, replica_groups=mesh['sp'=8,'tp'=4] {'sp'}, dimensions={0}, use_global_device_ids=true | all-gather | bytes 589824 | tf_op jit(solution)/shard_map/all_gather | solution.py:84
  58.3 10.0 %while.30 = (s32[]{:T(128)}, f32[128,4,64]{0,2,1:T(8,128)S(1)}, f32[4,128]{1,0:T(4,128)S(1)}, s32[]{:T(128)}, s32[]{:T(128)}, /*index=5*/bf16[1024,4,64]{0,2,1:T...) while((s32[]{:T(128)}, f32[128,4,64]{0,2,1:T(8,128)S(1)}, ...), condition=%wide.region_4.5_spmd.clone, body=%wide.region_0.4_spmd.clone.sunk | while | flops 109160584 | bytes 23688592 | solution.py:51
  58.6 1.9 fusion.106
  60.5 4.8 %fusion.107 = f32[4,128,4,128]{1,2,3,0:T(4,128)S(1)} fusion(f32[4,128,4,128]{1,3,2,0:T(8,128)S(1)} %bitcast.123), kind=kOutput, calls=%fused_computation.18.clone.1 | output fusion | flops 33292288 | bytes 2097152 | tf_op jit(solution)/shard_map/reduce-window.10
  68.7 2.5 fusion.71
  71.2 2.3 copy.75
  73.5 11.4 %while.31 = (s32[]{:T(128)}, f32[128,4,128]{0,2,1:T(8,128)S(1)}, f32[4,128]{1,0:T(4,128)S(1)}, s32[]{:T(128)}, s32[]{:T(128)}, /*index=5*/bf16[1024,4,128]{0,2,1...) while((s32[]{:T(128)}, f32[128,4,128]{0,2,1:T(8,128)S(1)}, ...), condition=%wide.region_9.10_spmd.clone, body=%wide.region_5.9_spmd.clone.sunk | while | flops 176302208 | bytes 22967640 | solution.py:51
  73.9 3.1 %fusion.114 = (f32[4,128]{1,0:T(4,128)S(1)}, f32[4,128,512]{1,2,0:T(8,128)S(1)}, f32[4,128,512]{1,2,0:T(8,128)}) fusion(pred[128,512]{0,1:T(8,128)(4,1)S(1)} %broadcast_compare_fusion.5, f32[4,512]{1,0:T(4,128)S(1)} %convert_bitcast_fusion.5, bf16[128,4,128]{2,0,1:T(8,128)(2,1)S(1)} %get-tuple-element.581, ...), kind=kOutput, calls=%fused_computation.59.clone.1 | convolution fusion | flops 69991936 | bytes 2828292 | tf_op jit(solution)/shard_map/while/body/qhd,khd->hqk/dot_general | solution.py:34
  77.0 4.8 %fusion.115 = f32[4,128,4,128]{1,2,3,0:T(4,128)S(1)} fusion(f32[4,128,4,128]{1,3,2,0:T(8,128)S(1)} %bitcast.124), kind=kOutput, calls=%fused_computation.47.clone.1 | output fusion | flops 33292288 | bytes 2097152 | tf_op jit(solution)/shard_map/reduce-window.12
  85.0 2.5 fusion.50
  89.3 53.1 %all-gather.9.cloned.1.call-done = bf16[512,2048]{1,0:T(8,128)(2,1)} async-done(((bf16[128,2048]{1,0:T(8,128)(2,1)}), bf16[512,2048]{1,0:T(8,128)(2,1)}) %all-gather.9.cloned.1.call-update) | async-done | bytes 2097168 | tf_op jit(solution)/shard_map/all_gather | solution.py:107
  142.4 2.0 reduce_sum.81
  146.2 53.7 %all_to_all.10 = bf16[8,64,2048]{2,1,0:T(8,128)(2,1)S(1)} all-to-all(bf16[8,64,2048]{2,1,0:T(8,128)(2,1)S(1)} %bitcast.126), channel_id=1, replica_groups=mesh['sp'=8,'tp'=4] {'sp'}, dimensions={0} | all-to-all | bytes 4194304 | tf_op jit(solution)/shard_map/all_to_all | solution.py:137
  199.9 2.3 fusion.44
  202.3 2.5 multiply_convert_fusion
  204.8 3.7 %fusion.46 = bf16[8,64,2048]{2,1,0:T(8,128)(2,1)} fusion(bf16[8,64,1024]{2,1,0:T(8,128)(2,1)S(1)} %bitcast.139, bf16[1,1024,2048]{2,1,0:T(8,128)(2,1)S(1)} %copy-done.24), kind=kOutput, calls=%fused_computation.66 | convolution fusion | flops 2148532224 | bytes 7340032 | tf_op jit(solution)/shard_map/dot_general | solution.py:148
  208.5 33.3 %reduce-scatter.3.cloned.1.call-done = bf16[8,16,2048]{2,1,0:T(8,128)(2,1)} async-done(((bf16[8,64,2048]{2,1,0:T(8,128)(2,1)}), bf16[8,16,2048]{2,1,0:T(8,128)(2,1)}) %reduce-scatter.3.cloned.1.call-update) | async-done | bytes 524304 | tf_op jit(solution)/shard_map/reduce_scatter | solution.py:151
  241.8 4.6 %all-to-all-start.1 = ((bf16[8,16,2048]{2,1,0:T(8,128)(2,1)}), bf16[8,16,2048]{2,1,0:T(8,128)(2,1)S(1)}, u32[]{:S(2)}, u32[]{:S(2)}) async-start(bf16[8,16,2048]{2,1,0:T(8,128)(2,1)} %reduce-scatter.3.cloned.1.call-done), calls=%async_computation.2 | async-start | bytes 1048576 | tf_op jit(solution)/shard_map/all_to_all | solution.py:154
  246.7 15.1 %all-to-all-done.1 = bf16[8,16,2048]{2,1,0:T(8,128)(2,1)S(1)} async-done(((bf16[8,16,2048]{2,1,0:T(8,128)(2,1)}), bf16[8,16,2048]{2,1,0:T(8,128)(2,1)S(1)}, u32[]{:S(2)}, u32[]{:S(2)}) %all-to-all-start.1) | async-done | bytes 524320 | tf_op jit(solution)/shard_map/all_to_all | solution.py:154
  263.4 23.2 %reduce-scatter.5.cloned.1.call-done = bf16[32,2048]{1,0:T(8,128)(2,1)} async-done(((bf16[128,2048]{1,0:T(8,128)(2,1)}), bf16[32,2048]{1,0:T(8,128)(2,1)}) %reduce-scatter.5.cloned.1.call-update) | async-done | bytes 131088 | tf_op jit(solution)/shard_map/reduce_scatter | solution.py:170
  288.9 1.7 add_convert_fusion.1
  (130 shorter events, 17.1 us)
Async XLA Ops:
  6.5 78.4 %copy-start = (bf16[512,2048]{1,0:T(8,128)(2,1)S(1)}, bf16[512,2048]{1,0:T(8,128)(2,1)}, u32[]{:S(2)}) copy-start(bf16[512,2048]{1,0:T(8,128)(2,1)} %param.32) | copy-start | bytes 6291460
  6.5 34.0 %copy-start.13 = (bf16[128,256]{1,0:T(8,128)(2,1)S(1)}, bf16[128,256]{1,0:T(8,128)(2,1)}, u32[]{:S(2)}) copy-start(bf16[128,256]{1,0:T(8,128)(2,1)} %param.26) | copy-start | bytes 196612
  6.5 64.7 %all-gather.5.cloned.1.call-start = ((), (), s32[]{:S(2)}) async-start(), calls=%async_computation.4 | async-start | bytes 1179648 | tf_op jit(solution)/shard_map/all_gather | solution.py:86
  7.3 66.3 %all-gather.7.cloned.1.call-start = ((), (), s32[]{:S(2)}) async-start(), calls=%async_computation.5 | async-start | bytes 1179648 | tf_op jit(solution)/shard_map/all_gather | solution.py:85
  9.0 133.4 %all-gather.9.cloned.1.call-start = ((), (), s32[]{:S(2)}) async-start(), calls=%async_computation.8 | async-start | bytes 2621440 | tf_op jit(solution)/shard_map/all_gather | solution.py:107
  58.3 10.1 %copy-start.10 = (bf16[128,512]{1,0:T(8,128)(2,1)S(1)}, bf16[128,512]{1,0:T(8,128)(2,1)}, u32[]{:S(2)}) copy-start(bf16[128,512]{1,0:T(8,128)(2,1)} %param.27) | copy-start | bytes 393220
  65.6 2.5 copy-start.4
  73.7 3.3 %copy-start.11 = (bf16[128,4,128]{2,0,1:T(8,128)(2,1)}, bf16[128,4,128]{2,0,1:T(8,128)(2,1)S(1)}, u32[]{:S(2)}) copy-start(bf16[128,4,128]{2,0,1:T(8,128)(2,1)S(1)} %get-tuple-element.581) | copy-start | bytes 393220 | tf_op jit(solution)/shard_map/while
  82.1 2.5 copy-start.3
  85.0 2.6 copy-start.20
  87.5 57.0 %copy-start.5 = (bf16[128,2048]{1,0:T(8,128)(2,1)S(1)}, bf16[128,2048]{1,0:T(8,128)(2,1)}, u32[]{:S(2)}) copy-start(bf16[128,2048]{1,0:T(8,128)(2,1)} %param.23) | copy-start | bytes 1572868
  87.5 154.3 %reduce-scatter.3.cloned.1.call-start = ((), (), s32[]{:S(2)}) async-start(), calls=%async_computation.6 | async-start | bytes 2621440 | tf_op jit(solution)/shard_map/reduce_scatter | solution.py:151
  142.4 2.7 copy-start.16
  142.4 2.7 copy-start.17
  145.4 54.5 %copy-start.6 = (bf16[128,2048]{1,0:T(8,128)(2,1)}, bf16[128,2048]{1,0:T(8,128)(2,1)S(1)}, u32[]{:S(2)}) copy-start(bf16[128,2048]{1,0:T(8,128)(2,1)S(1)} %add_convert_fusion) | copy-start | bytes 1572868
  146.2 53.7 %copy-start.22 = (bf16[1,2048,1024]{2,1,0:T(8,128)(2,1)S(1)}, bf16[1,2048,1024]{2,1,0:T(8,128)(2,1)}, u32[]{:S(2)}) copy-start(bf16[1,2048,1024]{2,1,0:T(8,128)(2,1)} %param.39) | copy-start | bytes 12582916
  199.9 2.4 copy-start.23
  202.2 2.5 copy-start.24
  208.5 38.1 %copy-start.21 = (f32[128,2]{0,1:T(2,128)S(1)}, f32[128,2]{0,1:T(2,128)}, u32[]{:S(2)}) copy-start(f32[128,2]{0,1:T(2,128)} %param.38) | copy-start | bytes 3076
  241.8 19.9 %all-to-all-start.1 = ((bf16[8,16,2048]{2,1,0:T(8,128)(2,1)}), bf16[8,16,2048]{2,1,0:T(8,128)(2,1)S(1)}, u32[]{:S(2)}, u32[]{:S(2)}) async-start(bf16[8,16,2048]{2,1,0:T(8,128)(2,1)} %reduce-scatter.3.cloned.1.call-done), calls=%async_computation.2 | async-start | bytes 1048576 | tf_op jit(solution)/shard_map/all_to_all | solution.py:154
  246.4 40.2 %reduce-scatter.5.cloned.1.call-start = ((), (), s32[]{:S(2)}) async-start(), calls=%async_computation.7 | async-start | bytes 655360 | tf_op jit(solution)/shard_map/reduce_scatter | solution.py:170
  261.8 24.9 %copy-start.7 = (bf16[128,2048]{1,0:T(8,128)(2,1)S(1)}, bf16[128,2048]{1,0:T(8,128)(2,1)}, u32[]{:S(2)}) copy-start(bf16[128,2048]{1,0:T(8,128)(2,1)} %copy-done.6) | copy-start | bytes 1572868
  261.8 27.1 %copy-start.18 = (f32[2048]{0:T(1024)S(1)}, f32[2048]{0:T(1024)}, u32[]{:S(2)}) copy-start(f32[2048]{0:T(1024)} %param.36) | copy-start | bytes 24580
  261.8 27.1 %copy-start.19 = (f32[2048]{0:T(1024)S(1)}, f32[2048]{0:T(1024)}, u32[]{:S(2)}) copy-start(f32[2048]{0:T(1024)} %param.35) | copy-start | bytes 24580
  (7 other events, 12.1 us)
Sparse Core Ops, SparseCore 0:
  8.9 27.5 all-gather.4
  38.1 26.5 all-gather.6
  87.6 54.7 all-gather.8
  208.6 33.1 reduce-scatter.2
  263.5 23.0 reduce-scatter.4
